TPU v7x, 32 devices: a whole 2x2x4 slice. The times are simulated.
32 devices in a mesh: sp: 8 (over z, x), tp: 4 (over y, core).
Axes of the slice: x: 2, y: 2, z: 4, core: 2. Of those that a mesh axis runs over, the one named last changes fastest.
Arguments:
- queries: bfloat16 [4096, 3072], P('sp', 'tp'), may hold values from -6 to 6
- latent: bfloat16 [4096, 1024], P('sp'), may hold values from -6 to 6
- rope_key: bfloat16 [4096, 64], P('sp'), may hold values from -6 to 6
- key_weight: bfloat16 [1024, 2048], P(None, 'tp'), as said below
- value_weight: bfloat16 [1024, 2048], P(None, 'tp'), as said below
- log_sums: float32 [16, 4096], P('tp', 'sp'), as said below
- attn_out: bfloat16 [4096, 2048], P('sp', 'tp'), as said below
- out_grad: bfloat16 [4096, 2048], P('sp', 'tp'), may hold values from -6 to 6
Outputs:
- d_queries: bfloat16 [4096, 3072], P('sp', 'tp')
- d_latent: float32 [4096, 1024], P('sp')
- d_rope: float32 [4096, 64], P('sp')
- d_value_weight: float32 [1024, 2048], P('sp', 'tp')
Inputs may be any that keep to these rules, and one draw needn't show every extreme that they name: `key_weight`: independent entries of order one multiplied by 1024^(-1/2). `value_weight`: independent entries of order one multiplied by 1024^(-1/2). log_sums[h, i] is the logarithm of the sum over j <= i of exp(scores[h, i, j]) of the forward pass. attn_out is the forward pass output: head h of row i is the sum over j <= i of exp(scores - log_sums) rounded to bfloat16, times head h of values row j, rounded to bfloat16.
All inputs are finite; a program needn't handle non-finite values.
Results may differ from a plain program's by a relative error of at most 0.018.
Values may be sent and summed in bfloat16 or wider, within the bound.
A program may use at most 192 MiB of HBM per device.

v0:
```python
import jax
import jax.numpy as jnp
from jax import lax
from jax.sharding import PartitionSpec as P

NOPE = 128
ROPE = 64
VDIM = 128


def score_block(
    query_nope,
    query_rope,
    grad_heads,
    lse_rows,
    delta_rows,
    key_heads,
    key_rope,
    value_heads,
    key_first,
):
    score_scale = (NOPE + ROPE) ** (-0.5)
    query_count = query_nope.shape[0]
    key_count = key_heads.shape[0]
    scores = score_scale * (
        jnp.einsum("qhn,khn->hqk", query_nope, key_heads, preferred_element_type=jnp.float32)
        + jnp.einsum("qhr,kr->hqk", query_rope, key_rope, preferred_element_type=jnp.float32)
    )
    query_pos = jnp.arange(query_count, dtype=jnp.int32)
    key_pos = key_first + jnp.arange(key_count, dtype=jnp.int32)
    causal = key_pos[None, :] <= query_pos[:, None]
    attn_probs = jnp.exp(jnp.where(causal[None], scores - lse_rows[:, :, None], -1e30))
    probs_b = attn_probs.astype(jnp.bfloat16)
    value_grad = jnp.einsum("hqk,qhv->khv", probs_b, grad_heads, preferred_element_type=jnp.float32)
    prob_grad = jnp.einsum(
        "qhv,khv->hqk", grad_heads, value_heads, preferred_element_type=jnp.float32
    )
    score_grad = (attn_probs * (prob_grad - delta_rows[:, :, None])).astype(jnp.bfloat16)
    query_grad = score_scale * jnp.concatenate(
        [
            jnp.einsum("hqk,khn->qhn", score_grad, key_heads, preferred_element_type=jnp.float32),
            jnp.einsum("hqk,kr->qhr", score_grad, key_rope, preferred_element_type=jnp.float32),
        ],
        axis=2,
    )
    key_grad = score_scale * jnp.einsum(
        "hqk,qhn->khn", score_grad, query_nope, preferred_element_type=jnp.float32
    )
    rope_grad = score_scale * jnp.einsum(
        "hqk,qhr->kr", score_grad, query_rope, preferred_element_type=jnp.float32
    )
    return (query_grad, key_grad, rope_grad, value_grad)


def keep_state(state_in):
    return state_in


def per_device(queries, latent, rope_key, key_weight, value_weight, log_sums, attn_out, out_grad):
    tok_rows = queries.shape[0]
    head_count = key_weight.shape[1] // NOPE
    head_width = NOPE + ROPE
    first_row = lax.axis_index("sp") * tok_rows
    total_rows = tok_rows * lax.axis_size("sp")
    grad_heads = out_grad.reshape(tok_rows, head_count, VDIM)
    out_heads = attn_out.reshape(tok_rows, head_count, VDIM)
    row_terms = jnp.sum(out_heads.astype(jnp.float32) * grad_heads.astype(jnp.float32), axis=2).T
    lse_all, delta_all = (
        lax.all_gather(log_sums, "sp", axis=1, tiled=True),
        lax.all_gather(row_terms, "sp", axis=1, tiled=True),
    )
    row_count = latent.shape[0]
    key_heads = (
        jnp.dot(latent, key_weight, preferred_element_type=jnp.float32)
        .astype(jnp.bfloat16)
        .reshape(row_count, head_count, NOPE)
    )
    value_heads = (
        jnp.dot(latent, value_weight, preferred_element_type=jnp.float32)
        .astype(jnp.bfloat16)
        .reshape(row_count, head_count, VDIM)
    )
    start_state = (
        jnp.zeros((tok_rows, head_count, NOPE), jnp.float32),
        jnp.zeros((tok_rows, ROPE), jnp.float32),
        jnp.zeros((tok_rows, head_count, VDIM), jnp.float32),
        jnp.zeros((total_rows, head_count * head_width), jnp.float32),
    )
    query_piece = lax.all_gather(queries, "sp", axis=0, tiled=True)
    grad_piece = lax.all_gather(out_grad, "sp", axis=0, tiled=True)
    piece_rows = query_piece.shape[0]

    def compute_piece(state_in):
        piece_heads = query_piece.reshape(piece_rows, head_count, head_width)
        query_grad, key_grad, rope_grad, value_grad = score_block(
            piece_heads[:, :, :NOPE],
            piece_heads[:, :, NOPE:],
            grad_piece.reshape(piece_rows, head_count, VDIM),
            lse_all,
            delta_all,
            key_heads,
            rope_key,
            value_heads,
            first_row,
        )
        query_buffer = query_grad.reshape(piece_rows, head_count * head_width)
        return (key_grad, rope_grad, value_grad, query_buffer)

    key_sum, rope_total, value_sum, query_buffer = lax.cond(
        jnp.int32(0) + piece_rows <= first_row, keep_state, compute_piece, start_state
    )
    query_total = lax.psum_scatter(
        query_buffer.astype(jnp.bfloat16), "sp", scatter_dimension=0, tiled=True
    )
    key_grad_b = key_sum.reshape(tok_rows, head_count * NOPE).astype(jnp.bfloat16)
    value_grad_b = value_sum.reshape(tok_rows, head_count * VDIM).astype(jnp.bfloat16)
    latent_part = jnp.dot(key_grad_b, key_weight.T, preferred_element_type=jnp.float32) + jnp.dot(
        value_grad_b, value_weight.T, preferred_element_type=jnp.float32
    )
    d_latent, d_rope = (
        lax.psum(latent_part.astype(jnp.bfloat16), "tp").astype(jnp.float32),
        lax.psum(rope_total.astype(jnp.bfloat16), "tp").astype(jnp.float32),
    )
    d_value_weight = lax.psum_scatter(
        lax.dot_general(
            latent, value_grad_b, (((0,), (0,)), ((), ())), preferred_element_type=jnp.float32
        ).astype(jnp.bfloat16),
        "sp",
        scatter_dimension=0,
        tiled=True,
    ).astype(jnp.float32)
    return (query_total, d_latent, d_rope, d_value_weight)


def solution(mesh):
    placed = (
        P("sp", "tp"),
        P("sp", None),
        P("sp", None),
        P(None, "tp"),
        P(None, "tp"),
        P("tp", "sp"),
        P("sp", "tp"),
        P("sp", "tp"),
    )
    return jax.shard_map(
        per_device,
        mesh=mesh,
        in_specs=placed,
        out_specs=(P("sp", "tp"), P("sp", None), P("sp", None), P("sp", "tp")),
        check_vma=False,
    )
```

profile of v0, /device:TPU:0, one launch (start us, length us, event | category | flops | bytes accessed | tf_op | source)
XLA Modules:
  0.0 581.1 jit_solution(2930090957411692504)
XLA Ops:
  7.2 2.1 copy.42
  9.4 2.3 copy.41
  11.8 1.3 convert_multiply_fusion
  14.2 33.2 %all_gather.13 = f32[4,4096]{1,0:T(4,128)S(1)} all-gather(f32[4,512]{1,0:T(4,128)S(1)} %copy-done.8), channel_id=1, replica_groups=mesh['sp'=8,'tp'=4] {'sp'}, dimensions={1}, use_global_device_ids=true | all-gather | bytes 73728 | tf_op jit(solution)/shard_map/all_gather | solution.py:69
  47.4 59.8 %all_gather.15 = f32[4,4096]{0,1:T(8,128)S(1)} all-gather(f32[4,512]{0,1:T(8,128)S(1)} %bitcast.72), channel_id=1, replica_groups=mesh['sp'=8,'tp'=4] {'sp'}, dimensions={1}, use_global_device_ids=true | all-gather | bytes 73728 | tf_op jit(solution)/shard_map/all_gather | solution.py:70
  107.2 2.7 convolution_convert_fusion.2
  110.0 2.7 convolution_convert_fusion.1
  112.7 9.5 %all-gather.5.cloned.1.call-done = bf16[4096,512]{0,1:T(8,128)(2,1)} async-done(((bf16[512,512]{0,1:T(8,128)(2,1)}), bf16[4096,512]{0,1:T(8,128)(2,1)}) %all-gather.5.cloned.1.call-update) | async-done | bytes 4194320 | tf_op jit(solution)/shard_map/all_gather | solution.py:90
  122.2 101.4 %all-gather.3.cloned.1.call-done = bf16[4096,768]{0,1:T(8,128)(2,1)} async-done(((bf16[512,768]{0,1:T(8,128)(2,1)}), bf16[4096,768]{0,1:T(8,128)(2,1)}) %all-gather.3.cloned.1.call-update) | async-done | bytes 6291472 | tf_op jit(solution)/shard_map/all_gather | solution.py:89
  223.6 121.5 %conditional.1 = (bf16[512,64]{0,1:T(8,128)(2,1)S(1)}, bf16[4096,768]{0,1:T(8,128)(2,1)}, bf16[512,512]{0,1:T(8,128)(2,1)}, bf16[512,512]{0,1:T(8,128)(2,1)}) conditional(s32[]{:T(128)} %convert_element_type.70, (s32[]{:T(128)}, bf16[4096,768]{0,1:T(8,128)(2,1)}, bf16[512,512]{1,0:T(8,128)(2,1)}, bf16[512,64]{0,1:T(8,128)(2,1)S(1)}, ...), branch_computations={%region_1.2_spmd, %region_2.3_spmd} | conditional | flops 14038138880 | bytes 400494752 | solution.py:109
  224.2 2.1 copy.43
  226.3 1.7 iota_compare_fusion
  228.0 17.9 %fusion.6 = f32[4,4096,512]{2,1,0:T(8,128)} fusion(bf16[512,4,128]{0,2,1:T(8,128)(2,1)} %bitcast.68, bf16[4096,4,192]{0,2,1:T(8,128)(2,1)} %bitcast.62), kind=kOutput, calls=%fused_computation.12 | convolution fusion | flops 2147483648 | bytes 38273024 | tf_op jit(solution)/shard_map/cond/branch_0_fun/qhn,khn->hqk/dot_general | solution.py:26
  245.9 27.6 %fusion.3 = f32[4,4096,512]{2,1,0:T(8,128)} fusion(f32[4,4096,512]{2,1,0:T(8,128)} %fusion.6, f32[4,4096]{1,0:T(4,128)S(1)} %get-tuple-element.24, pred[4096,512]{1,0:T(8,128)(4,1)S(1)} %iota_compare_fusion, bf16[4096,4,192]{0,2,1:T(8,128)(2,1)} %bitcast.63, bf16[512,64]{0,1:T(8,128)(2,1)S(1)} %get-tuple-element.41), kind=kOutput, calls=%fused_computation.4 | convolution fusion | flops 1107296256 | bytes 71434240 | tf_op jit(solution)/shard_map/cond/branch_0_fun/qhr,kr->hqk/dot_general | solution.py:27
  273.5 15.0 %fusion.19 = bf16[4,512,128]{1,2,0:T(8,128)(2,1)} fusion(bf16[4096,4,128]{0,2,1:T(8,128)(2,1)} %bitcast.66, f32[4,4096,512]{2,1,0:T(8,128)} %fusion.3), kind=kOutput, calls=%fused_computation.21 | convolution fusion | flops 2156134400 | bytes 38273024 | tf_op jit(solution)/shard_map/cond/branch_0_fun/hqk,qhv->khv/dot_general | solution.py:34
  288.6 19.1 %multiply_convert_fusion = bf16[4,4096,512]{2,1,0:T(8,128)(2,1)} fusion(f32[4,4096,512]{2,1,0:T(8,128)} %fusion.3, f32[4,4096]{1,0:T(4,128)S(1)} %copy.44, bf16[4096,4,128]{0,2,1:T(8,128)(2,1)} %bitcast.67, bf16[512,512]{1,0:T(8,128)(2,1)S(1)} %copy-done.5), kind=kOutput, calls=%fused_computation.5 | convolution fusion | flops 2172649472 | bytes 55115776 | tf_op jit(solution)/shard_map/cond/branch_0_fun/qhv,khv->hqk/dot_general | solution.py:35
  307.7 9.5 %fusion.25 = bf16[512,64]{0,1:T(8,128)(2,1)S(1)} fusion(bf16[4,4096,512]{2,1,0:T(8,128)(2,1)} %multiply_convert_fusion, bf16[4096,4,192]{0,2,1:T(8,128)(2,1)} %bitcast.64), kind=kOutput, calls=%fused_computation.23 | convolution fusion | flops 1073807360 | bytes 18939904 | tf_op jit(solution)/shard_map/cond/branch_0_fun/hqk,qhr->kr/dot_general | solution.py:49
  317.3 1.6 copy-done.1
  318.9 5.3 fusion.16
  324.2 7.1 %convolution_bitcast_fusion.1 = f32[4096,4,64]{0,2,1:T(8,128)} fusion(bf16[4,4096,512]{2,1,0:T(8,128)(2,1)S(1)} %copy-done.1, bf16[512,64]{0,1:T(8,128)(2,1)S(1)} %get-tuple-element.41), kind=kOutput, calls=%fused_computation.11 | convolution fusion | flops 1073741824 | bytes 21037056 | tf_op jit(solution)/shard_map/cond/branch_0_fun/hqk,kr->qhr/dot_general | solution.py:42
  331.3 9.2 %convolution_bitcast_fusion = f32[4096,4,128]{0,2,1:T(8,128)S(1)} fusion(bf16[4,4096,512]{2,1,0:T(8,128)(2,1)} %multiply_convert_fusion, bf16[512,4,128]{0,2,1:T(8,128)(2,1)S(1)} %bitcast.69), kind=kOutput, calls=%fused_computation.10 | convolution fusion | flops 2147483648 | bytes 25690112 | tf_op jit(solution)/shard_map/cond/branch_0_fun/hqk,khn->qhn/dot_general | solution.py:41
  340.5 4.5 maximum_multiply_fusion
  345.1 2.2 fusion.33
  347.3 3.2 add_convert_fusion
  351.2 1.3 copy.51
  352.6 8.7 %copy.45 = bf16[4096,768]{1,0:T(8,128)(2,1)} copy(bf16[4096,768]{0,1:T(8,128)(2,1)} %get-tuple-element.36) | data formatting | bytes 12582912 | tf_op jit(solution)/shard_map/cond | solution.py:109
  361.3 24.4 %all-reduce.3.cloned.1.call-done = (bf16[512,1024]{1,0:T(8,128)(2,1)}, bf16[512,64]{0,1:T(8,128)(2,1)}) async-done(((bf16[512,1024]{1,0:T(8,128)(2,1)}, bf16[512,64]{0,1:T(8,128)(2,1)}), (bf16[512,1024]{1,0:T(8,128)(2,1)}, bf16[512,64]{0,1:T(8,128)(2,1)})) %all-reduce.3.cloned.1.call-update) | async-done | bytes 1114128 | tf_op jit(solution)/shard_map/psum | solution.py:121
  385.7 1.5 convert_element_type.79
  387.2 2.8 convert_element_type.77
  390.0 63.6 %reduce-scatter.7.cloned.1.call-done = bf16[128,512]{1,0:T(8,128)(2,1)} async-done(((bf16[1024,512]{1,0:T(8,128)(2,1)}), bf16[128,512]{1,0:T(8,128)(2,1)}) %reduce-scatter.7.cloned.1.call-update) | async-done | bytes 131088
  453.6 1.0 copy.52
  455.4 119.1 %reduce-scatter.5.cloned.1.call-done = bf16[512,768]{1,0:T(8,128)(2,1)} async-done(((bf16[4096,768]{1,0:T(8,128)(2,1)}), bf16[512,768]{1,0:T(8,128)(2,1)}) %reduce-scatter.5.cloned.1.call-update) | async-done | bytes 786448 | tf_op jit(solution)/shard_map/reduce_scatter | solution.py:112
  (33 shorter events, 3.5 us)
Async XLA Ops:
  7.2 100.1 %copy-start = (bf16[512,1024]{1,0:T(8,128)(2,1)S(1)}, bf16[512,1024]{1,0:T(8,128)(2,1)}, u32[]{:S(2)}) copy-start(bf16[512,1024]{1,0:T(8,128)(2,1)} %param.11) | copy-start | bytes 3145732
  7.2 7.0 %copy-start.8 = (f32[4,512]{1,0:T(4,128)S(1)}, f32[4,512]{1,0:T(4,128)}, u32[]{:S(2)}) copy-start(f32[4,512]{1,0:T(4,128)} %param.15) | copy-start | bytes 24580
  7.2 115.0 %all-gather.5.cloned.1.call-start = ((), (), s32[]{:S(2)}) async-start(), calls=%async_computation.3 | async-start | bytes 4718592 | tf_op jit(solution)/shard_map/all_gather | solution.py:90
  9.4 214.2 %copy-start.7 = (bf16[512,64]{0,1:T(8,128)(2,1)S(1)}, bf16[512,64]{0,1:T(8,128)(2,1)}, u32[]{:S(2)}) copy-start(bf16[512,64]{0,1:T(8,128)(2,1)} %param.12) | copy-start | bytes 196612
  9.4 214.2 %all-gather.3.cloned.1.call-start = ((), (), s32[]{:S(2)}) async-start(), calls=%async_computation.2 | async-start | bytes 7077888 | tf_op jit(solution)/shard_map/all_gather | solution.py:89
  11.8 373.9 %all-reduce.3.cloned.1.call-start = ((), (), s32[]{:S(2)}) async-start(), calls=%async_computation.6 | async-start | bytes 2228224 | tf_op jit(solution)/shard_map/psum | solution.py:121
  273.5 15.0 %copy-start.5 = (bf16[512,512]{1,0:T(8,128)(2,1)S(1)}, bf16[512,512]{1,0:T(8,128)(2,1)}, u32[]{:S(2)}) copy-start(bf16[512,512]{1,0:T(8,128)(2,1)} %get-tuple-element.26) | copy-start | bytes 1572868 | tf_op jit(solution)/shard_map/cond
  307.7 11.2 %copy-start.1 = (bf16[4,4096,512]{2,1,0:T(8,128)(2,1)S(1)}, bf16[4,4096,512]{2,1,0:T(8,128)(2,1)}, u32[]{:S(2)}) copy-start(bf16[4,4096,512]{2,1,0:T(8,128)(2,1)} %multiply_convert_fusion) | copy-start | bytes 50331652 | tf_op jit(solution)/shard_map/cond
  324.2 7.1 %copy-start.3 = (bf16[512,512]{0,1:T(8,128)(2,1)S(1)}, bf16[512,512]{0,1:T(8,128)(2,1)}, u32[]{:S(2)}) copy-start(bf16[512,512]{0,1:T(8,128)(2,1)} %copy.43) | copy-start | bytes 1572868 | tf_op jit(solution)/shard_map/cond
  331.3 9.2 %copy-start.2 = (f32[4096,4,64]{0,2,1:T(8,128)S(1)}, f32[4096,4,64]{0,2,1:T(8,128)}, u32[]{:S(2)}) copy-start(f32[4096,4,64]{0,2,1:T(8,128)} %convolution_bitcast_fusion.1) | copy-start | bytes 12582916 | tf_op jit(solution)/shard_map/cond
  345.0 5.4 copy-start.6
  345.1 5.4 copy-start.4
  350.4 103.1 %reduce-scatter.7.cloned.1.call-start = ((), (), s32[]{:S(2)}) async-start(), calls=%async_computation.5 | async-start | bytes 1179648
  352.6 222.0 %reduce-scatter.5.cloned.1.call-start = ((), (), s32[]{:S(2)}) async-start(), calls=%async_computation.4 | async-start | bytes 7077888 | tf_op jit(solution)/shard_map/reduce_scatter | solution.py:112
Sparse Core Ops, SparseCore 0:
  10.0 112.0 all-gather.4
  124.8 98.7 all-gather.2
  350.6 35.0 all-reduce.2
  388.9 64.5 reduce-scatter.6
  457.6 116.9 reduce-scatter.4
where the time goes:
time: 582 us; the launch traced here: 581 us
  waiting for transfers between devices  318 us (55%)
  matrix products  122 us (21%)
  blocking collectives  93.1 us (16%)
  local copies, waits for them, and re-layouts  20.9 us (4%)
  between operations  13.9 us (2%)
  other arithmetic  12.5 us (2%)
    reduce_scatter x1, waiting for transfers between devices, per_device(): lax.psum_scatter(query_buffer.astype(jnp.bfloat16), 'sp', scatter_dimensi...  119 us
    all_gather x1, waiting for transfers between devices, per_device(): query_piece = lax.all_gather(queries, 'sp', axis=0, tiled=True)  101 us
    unnamed x6, waiting for transfers between devices  63.7 us
    all_gather x1, blocking collectives, per_device(): lax.all_gather(row_terms, 'sp', axis=1, tiled=True)  59.8 us
    all_gather x1, blocking collectives, per_device(): lax.all_gather(log_sums, 'sp', axis=1, tiled=True)  33.2 us
    dot_general x1, matrix products, score_block(): jnp.einsum('qhr,kr->hqk', query_rope, key_rope, preferred_element_type=jn...  27.6 us
    psum x1, waiting for transfers between devices, per_device(): lax.psum(latent_part.astype(jnp.bfloat16), 'tp').astype(jnp.float32)  24.4 us
    dot_general x1, matrix products, score_block(): jnp.einsum('qhv,khv->hqk', grad_heads, value_heads, preferred_element_typ...  19.1 us
  transfers between devices with their start and end apart: 5, of which 5 were waited for; matrix products, arithmetic and copies ran while one was open for 5% of the time, Pallas kernels for 0%

commit v1 on v0

v1 whole, which is shorter than its diff:
```python
import functools

import jax
import jax.numpy as jnp
from jax import lax
from jax.experimental import pallas as pl
from jax.experimental.pallas import tpu as pltpu
from jax.sharding import PartitionSpec as P

NOPE = 128
ROPE = 64
VDIM = 128
WIDE = 256
LOG2E = 1.4426950408889634
BF16 = jnp.bfloat16
F32 = jnp.float32


def dot_nn(a, b):
    return lax.dot_general(a, b, (((1,), (0,)), ((), ())), preferred_element_type=F32)


def dot_nt(a, b):
    return lax.dot_general(a, b, (((1,), (1,)), ((), ())), preferred_element_type=F32)


def attn_kernel(
    heads,
    latent_dim,
    mine_ref,
    q_ref,
    g_ref,
    lse_ref,
    delta_ref,
    lat_ref,
    wk_ref,
    wv_ref,
    dq_ref,
    dlat_ref,
    dvw_ref,
    q_s,
    qt_s,
    gt_s,
    dqt_s,
    kc_s,
    kct_s,
    v_s,
    dk_s,
    dv_s,
):
    j = pl.program_id(0)
    mine = mine_ref[0]
    rows = q_ref.shape[0]
    width = NOPE + ROPE
    scale = width ** (-0.5)

    @pl.when(j == 0)
    def _():
        for h in range(heads):
            qh = jnp.concatenate(
                [q_ref[:, h * width : (h + 1) * width], jnp.zeros((rows, WIDE - width), BF16)],
                axis=1,
            )
            q_s[h] = qh
            qt_s[h] = qh.T
            gt_s[h] = g_ref[:, h * VDIM : (h + 1) * VDIM].T
        dqt_s[...] = jnp.zeros_like(dqt_s)
        dvw_ref[...] = jnp.zeros_like(dvw_ref)

    @pl.when(j > mine)
    def _():
        dlat_ref[...] = jnp.zeros_like(dlat_ref)

    @pl.when(j <= mine)
    def _():
        lat = lat_ref[:, :latent_dim]
        rope = lat_ref[:, latent_dim:]
        keys = dot_nn(lat, wk_ref[...]).astype(BF16)
        v_s[...] = dot_nn(lat, wv_ref[...]).astype(BF16)
        for h in range(heads):
            kc = jnp.concatenate([keys[:, h * NOPE : (h + 1) * NOPE], rope], axis=1)
            kc_s[h] = kc
            kct_s[h] = kc.T
        rope_sum = jnp.zeros((rows, WIDE - NOPE), F32)
        k_pos = lax.broadcasted_iota(jnp.int32, (rows, rows), 0)
        q_pos = lax.broadcasted_iota(jnp.int32, (rows, rows), 1)
        causal = k_pos - q_pos <= (mine - j) * rows
        for h in range(heads):
            s = dot_nn(kc_s[h], qt_s[h])
            z = s * (scale * LOG2E) - lse_ref[h : h + 1, :] * LOG2E
            p = jnp.exp2(jnp.where(causal, z, -1e30))
            dp = dot_nn(v_s[:, h * VDIM : (h + 1) * VDIM], gt_s[h])
            ds = (p * (dp - delta_ref[h : h + 1, :])).astype(BF16)
            dv_s[:, h * VDIM : (h + 1) * VDIM] = dot_nn(
                p.astype(BF16), g_ref[:, h * VDIM : (h + 1) * VDIM]
            ).astype(BF16)
            dk = scale * dot_nn(ds, q_s[h])
            dk_s[:, h * NOPE : (h + 1) * NOPE] = dk[:, :NOPE].astype(BF16)
            rope_sum = rope_sum + dk[:, NOPE:]
            dqt_s[h] += dot_nn(kct_s[h], ds)
        dlat = dot_nt(dk_s[...], wk_ref[...]) + dot_nt(dv_s[...], wv_ref[...])
        dlat_ref[:, :latent_dim] = dlat.astype(BF16)
        dlat_ref[:, latent_dim:] = rope_sum.astype(BF16)
        dvw_ref[...] += dot_nn(lat.T, dv_s[...])

    @pl.when(j == pl.num_programs(0) - 1)
    def _():
        for h in range(heads):
            dq_ref[:, h * width : (h + 1) * width] = (
                (scale * dqt_s[h]).T[:, :width].astype(BF16)
            )


def attn_backward(mine, queries, out_grad, lse, delta, lat_all, key_weight, value_weight):
    rows = queries.shape[0]
    latent_dim = key_weight.shape[0]
    heads = key_weight.shape[1] // NOPE
    blocks = lat_all.shape[0] // rows
    packed = lat_all.shape[1]

    def whole(j, m):
        return (0, 0)

    return pl.pallas_call(
        functools.partial(attn_kernel, heads, latent_dim),
        grid_spec=pltpu.PrefetchScalarGridSpec(
            num_scalar_prefetch=1,
            grid=(blocks,),
            in_specs=[
                pl.BlockSpec(queries.shape, whole),
                pl.BlockSpec(out_grad.shape, whole),
                pl.BlockSpec(lse.shape, whole),
                pl.BlockSpec(delta.shape, whole),
                pl.BlockSpec((rows, packed), lambda j, m: (jnp.minimum(j, m[0]), 0)),
                pl.BlockSpec(key_weight.shape, whole),
                pl.BlockSpec(value_weight.shape, whole),
            ],
            out_specs=[
                pl.BlockSpec(queries.shape, whole),
                pl.BlockSpec((rows, packed), lambda j, m: (j, 0)),
                pl.BlockSpec(value_weight.shape, whole),
            ],
            scratch_shapes=[
                pltpu.VMEM((heads, rows, WIDE), BF16),
                pltpu.VMEM((heads, WIDE, rows), BF16),
                pltpu.VMEM((heads, VDIM, rows), BF16),
                pltpu.VMEM((heads, WIDE, rows), F32),
                pltpu.VMEM((heads, rows, WIDE), BF16),
                pltpu.VMEM((heads, WIDE, rows), BF16),
                pltpu.VMEM((rows, heads * VDIM), BF16),
                pltpu.VMEM((rows, heads * NOPE), BF16),
                pltpu.VMEM((rows, heads * VDIM), BF16),
            ],
        ),
        out_shape=[
            jax.ShapeDtypeStruct(queries.shape, BF16),
            jax.ShapeDtypeStruct(lat_all.shape, BF16),
            jax.ShapeDtypeStruct(value_weight.shape, F32),
        ],
        compiler_params=pltpu.CompilerParams(
            dimension_semantics=("arbitrary",), vmem_limit_bytes=60 * 1024 * 1024
        ),
    )(mine, queries, out_grad, lse, delta, lat_all, key_weight, value_weight)


def per_device(queries, latent, rope_key, key_weight, value_weight, log_sums, attn_out, out_grad):
    rows, latent_dim = latent.shape
    heads = key_weight.shape[1] // NOPE
    tp = lax.axis_size("tp")
    mine = lax.axis_index("sp").astype(jnp.int32).reshape((1,))
    row_terms = jnp.sum(
        attn_out.reshape(rows, heads, VDIM).astype(F32)
        * out_grad.reshape(rows, heads, VDIM).astype(F32),
        axis=2,
    ).T
    part = rows // tp
    start = lax.axis_index("tp") * part
    lat_piece = lax.dynamic_slice_in_dim(latent, start, part, 0)
    rope_piece = lax.dynamic_slice_in_dim(rope_key, start, part, 0)
    piece = jnp.concatenate(
        [lat_piece, rope_piece, jnp.zeros((part, WIDE - NOPE - ROPE), BF16)], axis=1
    )
    lat_all = lax.all_gather(piece, ("sp", "tp"), axis=0, tiled=True)
    d_queries, dlat, dvw = attn_backward(
        mine, queries, out_grad, log_sums, row_terms, lat_all, key_weight, value_weight
    )
    dlat_piece = lax.psum_scatter(dlat, ("sp", "tp"), scatter_dimension=0, tiled=True)
    d_value_weight = lax.psum_scatter(
        dvw.astype(BF16), "sp", scatter_dimension=0, tiled=True
    ).astype(F32)
    dlat_own = lax.all_gather(dlat_piece, "tp", axis=0, tiled=True)
    d_latent = dlat_own[:, :latent_dim].astype(F32)
    d_rope = dlat_own[:, latent_dim : latent_dim + ROPE].astype(F32)
    return (d_queries, d_latent, d_rope, d_value_weight)


def solution(mesh):
    placed = (
        P("sp", "tp"),
        P("sp", None),
        P("sp", None),
        P(None, "tp"),
        P(None, "tp"),
        P("tp", "sp"),
        P("sp", "tp"),
        P("sp", "tp"),
    )
    return jax.shard_map(
        per_device,
        mesh=mesh,
        in_specs=placed,
        out_specs=(P("sp", "tp"), P("sp", None), P("sp", None), P("sp", "tp")),
        check_vma=False,
    )
```

time: 582 us -> 380 us (0.65)
  matrix products: 122 us -> 0 us
  blocking collectives: 93.1 us -> 0 us
  waiting for transfers between devices: 318 us -> 336 us
  local copies, waits for them, and re-layouts: 20.9 us -> 5.38 us
  Pallas kernels: 0 us -> 15.2 us
    dot_general x13 -> x0, matrix products: 122 us -> none  [the longest x1 27.6 us: score_block(): jnp.einsum('qhr,kr->hqk', query_rope, key_rope, preferred_element_type=jn...]
    reduce_scatter x1 -> x2, waiting for transfers between devices: 119 us -> 237 us  [the longest x1 170 us: per_device(): lax.psum_scatter(dlat, ('sp', 'tp'), scatter_dimension=0, tiled=True)]
    all_gather x2 -> x0, blocking collectives: 93.1 us -> none  [the longest x1 59.8 us: per_device(): lax.all_gather(row_terms, 'sp', axis=1, tiled=True)]
    unnamed x6 -> x4, waiting for transfers between devices: 63.7 us -> 0.07 us
    psum x1 -> x0, waiting for transfers between devices: 24.4 us -> none  [per_device(): lax.psum(latent_part.astype(jnp.bfloat16), 'tp').astype(jnp.float32)]
    pallas_call x0 -> x1, Pallas kernels: none -> 15.2 us  [attn_backward(): pl.pallas_call(functools.partial(attn_kernel, heads, latent_dim), grid_sp...]
    all_gather x2, waiting for transfers between devices: 111 us -> 99.4 us  [the longest x1 83.3 us: per_device(): lat_all = lax.all_gather(piece, ('sp', 'tp'), axis=0, tiled=True)]
    cond x9 -> x0, local copies, waits for them, and re-layouts: 10.3 us -> none  [the longest x1 8.68 us: per_device(): lax.cond(jnp.int32(0) + piece_rows <= first_row, keep_state, compute_piec...]
  transfers between devices with their start and end apart: 5 -> 4, of which waited for: 5 -> 4; matrix products, arithmetic and copies ran while one was open for 5% -> 2% of each run, Pallas kernels for 0% -> 0%
where the time goes in v1:
time: 380 us; the launch traced here: 379 us
  waiting for transfers between devices  336 us (88%)
  Pallas kernels  15.2 us (4%)
  between operations  13.8 us (4%)
  other arithmetic  8.4 us (2%)
  local copies, waits for them, and re-layouts  5.38 us (1%)
    reduce_scatter x1, waiting for transfers between devices, per_device(): lax.psum_scatter(dlat, ('sp', 'tp'), scatter_dimension=0, tiled=True)  170 us
    all_gather x1, waiting for transfers between devices, per_device(): lat_all = lax.all_gather(piece, ('sp', 'tp'), axis=0, tiled=True)  83.3 us
    reduce_scatter x1, waiting for transfers between devices, per_device(): lax.psum_scatter(dvw.astype(BF16), 'sp', scatter_dimension=0, tiled=True)  67.1 us
    all_gather x1, waiting for transfers between devices, per_device(): dlat_own = lax.all_gather(dlat_piece, 'tp', axis=0, tiled=True)  16.2 us
    pallas_call x1, Pallas kernels, attn_backward(): pl.pallas_call(functools.partial(attn_kernel, heads, latent_dim), grid_sp...  15.2 us
  transfers between devices with their start and end apart: 4, of which 4 were waited for; matrix products, arithmetic and copies ran while one was open for 2% of the time, Pallas kernels for 0%

profile of v1, /device:TPU:0, one launch (start us, length us, event | category | flops | bytes accessed | tf_op | source)
XLA Modules:
  0.0 379.5 jit_solution(1563819959099579274)
XLA Ops:
  7.2 0.0 copy-start
  7.2 0.0 all-gather.3.cloned.1.call-start
  7.2 0.8 constant_dynamic-slice_fusion
  8.0 0.1 copy.17
  8.2 0.3 copy-done
  8.4 0.8 concatenate.3
  9.3 0.0 all-gather.3.cloned.1.call-update
  9.3 0.0 reduce-scatter.3.cloned.1.call-start
  9.3 1.3 convert_multiply_fusion
  10.7 0.4 mul.10
  11.1 0.6 reduce_sum.9
  11.7 0.7 copy.14
  12.4 83.3 %all-gather.3.cloned.1.call-done.lat_ref = bf16[4096,1152]{1,0:T(8,128)(2,1)} async-done(((bf16[128,1152]{1,0:T(8,128)(2,1)}), bf16[4096,1152]{1,0:T(8,128)(2,1)}) %all-gather.3.cloned.1.call-update) | async-done | bytes 9437200 | tf_op jit(solution)/shard_map/all_gather | solution.py:183
  95.7 15.2 %shard_map.111 = (bf16[512,768]{1,0:T(8,128)(2,1)}, bf16[4096,1152]{1,0:T(8,128)(2,1)}, f32[1024,512]{1,0:T(8,128)}) custom-call(s32[1]{0:T(128)} %bitcast.mine_ref, bf16[512,768]{1,0:T(8,128)(2,1)} %q_ref.1, bf16[512,512]{1,0:T(8,128)(2,1)} %g_ref.1, f32[4,512]{1,0:T(4,128)} %lse_ref.1, f32[4,512]{1,0:T(4,128)} %bitcast.2, ...), custom_call_target="tpu_custom_call" | custom-call | tf_op jit(solution)/shard_map/pallas_call | solution.py:124
  110.9 0.0 copy-start.1
  110.9 0.0 reduce-scatter.3.cloned.1.call-update
  110.9 0.0 reduce-scatter.5.cloned.1.call-start
  111.0 1.5 copy-done.1
  112.5 1.1 convert_element_type.24
  113.6 0.0 reduce-scatter.5.cloned.1.call-update
  113.6 0.0 all-gather.5.cloned.1.call-start
  113.7 169.8 %reduce-scatter.3.cloned.1.call-done = bf16[128,1152]{1,0:T(8,128)(2,1)} async-done(((bf16[4096,1152]{1,0:T(8,128)(2,1)}), bf16[128,1152]{1,0:T(8,128)(2,1)}) %reduce-scatter.3.cloned.1.call-update) | async-done | bytes 294928 | tf_op jit(solution)/shard_map/reduce_scatter | solution.py:187
  283.5 0.0 all-gather.5.cloned.1.call-update
  283.5 67.1 %reduce-scatter.5.cloned.1.call-done = bf16[128,512]{1,0:T(8,128)(2,1)} async-done(((bf16[1024,512]{1,0:T(8,128)(2,1)}), bf16[128,512]{1,0:T(8,128)(2,1)}) %reduce-scatter.5.cloned.1.call-update) | async-done | bytes 131088 | tf_op jit(solution)/shard_map/reduce_scatter | solution.py:188
  350.7 1.6 convert_element_type.25
  352.3 16.2 %all-gather.5.cloned.1.call-done = bf16[512,1152]{1,0:T(8,128)(2,1)} async-done(((bf16[128,1152]{1,0:T(8,128)(2,1)}), bf16[512,1152]{1,0:T(8,128)(2,1)}) %all-gather.5.cloned.1.call-update) | async-done | bytes 1179664 | tf_op jit(solution)/shard_map/all_gather | solution.py:191
  368.5 0.9 slice_convert_fusion.1
  369.4 0.8 copy.16
  370.2 2.8 slice_convert_fusion
  (2 shorter events, 0.0 us)
Async XLA Ops:
  7.2 1.2 copy-start
  7.2 88.5 %all-gather.3.cloned.1.call-start = ((), (), s32[]{:S(2)}) async-start(), calls=%async_computation.2 | async-start | bytes 9732096 | tf_op jit(solution)/shard_map/all_gather | solution.py:183
  9.3 274.2 %reduce-scatter.3.cloned.1.call-start = ((), (), s32[]{:S(2)}) async-start(), calls=%async_computation.3 | async-start | bytes 9732096 | tf_op jit(solution)/shard_map/reduce_scatter | solution.py:187
  110.9 1.6 copy-start.1
  110.9 239.7 %reduce-scatter.5.cloned.1.call-start = ((), (), s32[]{:S(2)}) async-start(), calls=%async_computation.5 | async-start | bytes 1179648 | tf_op jit(solution)/shard_map/reduce_scatter | solution.py:188
  113.6 254.8 %all-gather.5.cloned.1.call-start = ((), (), s32[]{:S(2)}) async-start(), calls=%async_computation.4 | async-start | bytes 1474560 | tf_op jit(solution)/shard_map/all_gather | solution.py:191
Sparse Core Ops, SparseCore 0:
  11.5 84.1 all-gather.2
  111.0 172.4 reduce-scatter.2
  287.5 63.1 reduce-scatter.4
  352.1 16.3 all-gather.4

commit v2 on v1

--- a/solution.py
+++ b/solution.py
@@ -185,9 +185,11 @@
         mine, queries, out_grad, log_sums, row_terms, lat_all, key_weight, value_weight
     )
     dlat_piece = lax.psum_scatter(dlat, ("sp", "tp"), scatter_dimension=0, tiled=True)
-    d_value_weight = lax.psum_scatter(
-        dvw.astype(BF16), "sp", scatter_dimension=0, tiled=True
-    ).astype(F32)
+    sp = lax.axis_size("sp")
+    dvw_parts = lax.all_to_all(dvw.astype(BF16), "sp", 0, 0, tiled=True)
+    d_value_weight = jnp.sum(
+        dvw_parts.reshape(sp, latent_dim // sp, dvw.shape[1]).astype(F32), axis=0
+    )
     dlat_own = lax.all_gather(dlat_piece, "tp", axis=0, tiled=True)
     d_latent = dlat_own[:, :latent_dim].astype(F32)
     d_rope = dlat_own[:, latent_dim : latent_dim + ROPE].astype(F32)

time: 380 us -> 313 us (0.82)
  waiting for transfers between devices: 336 us -> 229 us
  starting transfers between devices: 0.16 us -> 41.8 us
    reduce_scatter x1 -> x0, waiting for transfers between devices: 67.1 us -> none  [per_device(): lax.psum_scatter(dvw.astype(BF16), 'sp', scatter_dimension=0, tiled=True)]
    all_to_all x0 -> x1, starting transfers between devices: none -> 41.7 us  [per_device(): dvw_parts = lax.all_to_all(dvw.astype(BF16), 'sp', 0, 0, tiled=True)]
    reduce_scatter x1, waiting for transfers between devices: 170 us -> 128 us  [per_device(): lax.psum_scatter(dlat, ('sp', 'tp'), scatter_dimension=0, tiled=True)]
  transfers between devices with their start and end apart: 4 -> 4, of which waited for: 4 -> 3; matrix products, arithmetic and copies ran while one was open for 2% -> 2% of each run, Pallas kernels for 0% -> 0%
where the time goes in v2:
time: 313 us
  waiting for transfers between devices  229 us (73%)
  starting transfers between devices  41.8 us (13%)
  Pallas kernels  15.2 us (5%)
  between operations  13.8 us (4%)
  other arithmetic  7.62 us (2%)
  local copies, waits for them, and re-layouts  5.43 us (2%)
    reduce_scatter x1, waiting for transfers between devices, per_device(): lax.psum_scatter(dlat, ('sp', 'tp'), scatter_dimension=0, tiled=True)  128 us
    all_gather x1, waiting for transfers between devices, per_device(): lat_all = lax.all_gather(piece, ('sp', 'tp'), axis=0, tiled=True)  83.3 us
    all_to_all x1, starting transfers between devices, per_device(): dvw_parts = lax.all_to_all(dvw.astype(BF16), 'sp', 0, 0, tiled=True)  41.7 us
    all_gather x1, waiting for transfers between devices, per_device(): dlat_own = lax.all_gather(dlat_piece, 'tp', axis=0, tiled=True)  17.1 us
    pallas_call x1, Pallas kernels, attn_backward(): pl.pallas_call(functools.partial(attn_kernel, heads, latent_dim), grid_sp...  15.2 us
  transfers between devices with their start and end apart: 4, of which 3 were waited for; matrix products, arithmetic and copies ran while one was open for 2% of the time, Pallas kernels for 0%

profile of v2, /device:TPU:0, one launch (start us, length us, event | category | flops | bytes accessed | tf_op | source)
XLA Modules:
  0.0 312.5 jit_solution(7623646440613211574)
XLA Ops:
  7.2 0.0 copy-start
  7.2 0.0 all-gather.3.cloned.1.call-start
  7.2 0.8 constant_dynamic-slice_fusion
  8.0 0.1 copy.17
  8.2 0.3 copy-done
  8.4 0.8 concatenate.3
  9.3 0.0 all-gather.3.cloned.1.call-update
  9.3 0.0 reduce-scatter.2.cloned.1.call-start
  9.3 1.3 convert_multiply_fusion
  10.7 0.4 mul.10
  11.1 0.6 reduce_sum.18
  11.7 0.7 copy.14
  12.4 83.3 %all-gather.3.cloned.1.call-done.lat_ref = bf16[4096,1152]{1,0:T(8,128)(2,1)} async-done(((bf16[128,1152]{1,0:T(8,128)(2,1)}), bf16[4096,1152]{1,0:T(8,128)(2,1)}) %all-gather.3.cloned.1.call-update) | async-done | bytes 9437200 | tf_op jit(solution)/shard_map/all_gather | solution.py:183
  95.7 15.2 %shard_map.111 = (bf16[512,768]{1,0:T(8,128)(2,1)}, bf16[4096,1152]{1,0:T(8,128)(2,1)}, f32[1024,512]{1,0:T(8,128)}) custom-call(s32[1]{0:T(128)} %bitcast.mine_ref, bf16[512,768]{1,0:T(8,128)(2,1)} %q_ref.1, bf16[512,512]{1,0:T(8,128)(2,1)} %g_ref.1, f32[4,512]{1,0:T(4,128)} %lse_ref.1, f32[4,512]{1,0:T(4,128)} %bitcast.3, ...), custom_call_target="tpu_custom_call" | custom-call | tf_op jit(solution)/shard_map/pallas_call | solution.py:124
  110.9 0.0 copy-start.1
  110.9 0.0 reduce-scatter.2.cloned.1.call-update
  110.9 1.6 copy-done.1
  112.5 1.1 convert_element_type.24
  113.6 41.7 %all-to-all-start = ((bf16[8,128,512]{2,1,0:T(8,128)(2,1)}), bf16[8,128,512]{2,1,0:T(8,128)(2,1)S(1)}, u32[]{:S(2)}, u32[]{:S(2)}) async-start(bf16[8,128,512]{2,1,0:T(8,128)(2,1)} %bitcast.2), calls=%async_computation.1 | async-start | bytes 2097152 | tf_op jit(solution)/shard_map/all_to_all | solution.py:189
  155.3 0.0 all-gather.5.cloned.1.call-start
  155.3 128.2 %reduce-scatter.2.cloned.1.call-done = bf16[128,1152]{1,0:T(8,128)(2,1)} async-done(((bf16[4096,1152]{1,0:T(8,128)(2,1)}), bf16[128,1152]{1,0:T(8,128)(2,1)}) %reduce-scatter.2.cloned.1.call-update) | async-done | bytes 294928 | tf_op jit(solution)/shard_map/reduce_scatter | solution.py:187
  283.5 0.0 all-gather.5.cloned.1.call-update
  283.5 0.0 all-to-all-done
  283.5 0.8 convert_reduce_fusion
  284.4 17.1 %all-gather.5.cloned.1.call-done = bf16[512,1152]{1,0:T(8,128)(2,1)} async-done(((bf16[128,1152]{1,0:T(8,128)(2,1)}), bf16[512,1152]{1,0:T(8,128)(2,1)}) %all-gather.5.cloned.1.call-update) | async-done | bytes 1179664 | tf_op jit(solution)/shard_map/all_gather | solution.py:193
  301.5 0.9 slice_convert_fusion.1
  302.4 0.8 copy.16
  303.2 2.8 slice_convert_fusion
  (2 shorter events, 0.0 us)
Async XLA Ops:
  7.2 1.2 copy-start
  7.2 88.5 %all-gather.3.cloned.1.call-start = ((), (), s32[]{:S(2)}) async-start(), calls=%async_computation.2 | async-start | bytes 9732096 | tf_op jit(solution)/shard_map/all_gather | solution.py:183
  9.3 274.2 %reduce-scatter.2.cloned.1.call-start = ((), (), s32[]{:S(2)}) async-start(), calls=%async_computation.3 | async-start | bytes 9732096 | tf_op jit(solution)/shard_map/reduce_scatter | solution.py:187
  110.9 1.6 copy-start.1
  113.6 169.9 %all-to-all-start = ((bf16[8,128,512]{2,1,0:T(8,128)(2,1)}), bf16[8,128,512]{2,1,0:T(8,128)(2,1)S(1)}, u32[]{:S(2)}, u32[]{:S(2)}) async-start(bf16[8,128,512]{2,1,0:T(8,128)(2,1)} %bitcast.2), calls=%async_computation.1 | async-start | bytes 2097152 | tf_op jit(solution)/shard_map/all_to_all | solution.py:189
  155.3 146.2 %all-gather.5.cloned.1.call-start = ((), (), s32[]{:S(2)}) async-start(), calls=%async_computation.4 | async-start | bytes 1474560 | tf_op jit(solution)/shard_map/all_gather | solution.py:193
Sparse Core Ops, SparseCore 0:
  11.5 84.1 all-gather.2
  111.0 172.4 reduce-scatter.1
  285.1 16.3 all-gather.4
